TPU v7x, 128 devices: a whole 4x4x4 slice. The times are simulated.
128 devices in a mesh: tp: 16 (over z, y), dp: 8 (over x, core).
Axes of the slice: x: 4, y: 4, z: 4, core: 2. Of those that a mesh axis runs over, the one named last changes fastest.
Arguments:
- tokens: bfloat16 [256, 4096], P('dp', 'tp'), may hold values from -6 to 6
- lengths: int32 [256], P('dp'), may hold values from 1 to 96, 6144 in all
- norm_gain: float32 [2, 4096], replicated, may hold values from 0.1 to 1.9
- w_recept: bfloat16 [2, 4096, 4096], P(None, None, ('tp', 'dp')), may hold values from -0.09375 to 0.09375
- w_key: bfloat16 [2, 4096, 4096], P(None, None, ('tp', 'dp')), may hold values from -0.09375 to 0.09375
- w_value: bfloat16 [2, 4096, 4096], P(None, None, ('tp', 'dp')), may hold values from -0.09375 to 0.09375
- w_decay: bfloat16 [2, 4096, 4096], P(None, None, ('tp', 'dp')), may hold values from -0.09375 to 0.09375
- w_rate: bfloat16 [2, 4096, 4096], P(None, None, ('tp', 'dp')), may hold values from -0.09375 to 0.09375
- w_gate: bfloat16 [2, 4096, 4096], P(None, None, ('tp', 'dp')), may hold values from -0.09375 to 0.09375
- w_out: bfloat16 [2, 4096, 4096], P(None, None, ('tp', 'dp')), may hold values from -0.09375 to 0.09375
- decay_base: float32 [2, 4096], P(None, 'tp'), may hold values from -3 to 1
- rate_base: float32 [2, 4096], P(None, 'tp'), may hold values from -3 to 3
- group_gain: float32 [2, 4096], P(None, 'tp'), may hold values from 0.1 to 1.9
- state: float32 [2, 256, 64, 64, 64], P(None, 'dp', 'tp'), may hold values from -6 to 6
Outputs:
- mixed: bfloat16 [256, 4096], P('dp', 'tp')
- new_state: float32 [2, 256, 64, 64, 64], P(None, 'dp', 'tp')
Inputs may be any that keep to these rules, and one draw needn't show every extreme that they name: Each sequence's live length lies between 1 and 96, some sequences reach 96, and the lengths sum to 6144.
All inputs are finite; a program needn't handle non-finite values.
Results may differ from a plain program's by a relative error of at most 0.025.
Values may be sent and summed in bfloat16 or wider, within the bound.
A program may use at most 128 MiB of HBM per device.

v0:
```python
import jax
import jax.numpy as jnp
from jax import lax
from jax.sharding import Mesh
from jax.sharding import PartitionSpec as P

STEP = 16
TP = ("tp_0", "tp_1")
TP_DP = ("tp_0", "tp_1", "dp")


RMS_EPS = 1e-06
GROUP_EPS = 0.00064


def gather_axes(value, axes, dim):
    if not axes:
        return value
    nearer = lax.all_gather(value, axes[-1], axis=dim, tiled=True)
    return gather_axes(nearer, axes[:-1], dim)


def shortened(value):
    def short(part):
        return part.astype(jnp.bfloat16) if part.dtype == jnp.float32 else part

    return jax.tree.map(short, value)


def over_axes(value, axes, dim, absorb, carry):
    everything = jax.tree.map(lambda part: gather_axes(part, axes, dim), value)
    return absorb(carry, everything, jnp.int32(0))


def recur(state_old, recept, key_vec, value_vec, decay_rate, learn_rate, active, head_size):
    split = (recept.shape[0], -1, head_size)
    recept_h = recept.reshape(split)
    key_h = key_vec.reshape(split)
    value_h = value_vec.reshape(split)
    decay_h = decay_rate.reshape(split)
    rate_h = learn_rate.reshape(split)
    key_len = jnp.sqrt(jnp.sum(key_h * key_h, axis=-1, keepdims=True))
    key_unit = key_h / jnp.maximum(key_len, 1e-12)
    state_a = jnp.einsum("bhij,bhj->bhi", state_old, -key_unit, precision=lax.Precision.DEFAULT)
    updated = (
        state_old * decay_h[:, :, None, :]
        + state_a[:, :, :, None] * (key_unit * rate_h)[:, :, None, :]
        + value_h[:, :, :, None] * (key_h * rate_h)[:, :, None, :]
    )
    updated = jnp.where(active[:, None, None, None], updated, state_old)
    readout = jnp.einsum("bhij,bhj->bhi", updated, recept_h, precision=lax.Precision.DEFAULT)
    centre = jnp.mean(readout, axis=-1, keepdims=True)
    spread = jnp.mean(jnp.square(readout - centre), axis=-1, keepdims=True)
    normal_out = ((readout - centre) * lax.rsqrt(spread + GROUP_EPS)).reshape(recept.shape[0], -1)
    return (updated, normal_out)


def local(
    tokens,
    lengths,
    norm_gain,
    w_recept,
    w_key,
    w_value,
    w_decay,
    w_rate,
    w_gate,
    w_out,
    decay_base,
    rate_base,
    group_gain,
    state,
):
    slim = w_recept.shape[2]
    head_size = state.shape[-1]
    active = lengths > STEP
    current = tokens
    updated_states = []
    for layer_idx in range(2):
        joined = jnp.concatenate(
            [
                w_recept[layer_idx],
                w_key[layer_idx],
                w_value[layer_idx],
                w_decay[layer_idx],
                w_rate[layer_idx],
                w_gate[layer_idx],
            ],
            axis=1,
        )
        batch_raw = lax.all_gather(current, "dp", axis=0, tiled=True)
        every_feature = gather_axes(batch_raw, TP, 1)
        values = every_feature.astype(jnp.float32)
        factor = lax.rsqrt(jnp.mean(values * values, axis=1, keepdims=True) + RMS_EPS)
        normed = (values * factor * norm_gain[layer_idx]).astype(jnp.bfloat16)
        projected = jnp.dot(normed, joined, preferred_element_type=jnp.float32)
        pieces = [
            projected[:, idx * slim : (idx + 1) * slim].astype(jnp.bfloat16) for idx in range(6)
        ]
        arrived = (
            lax.all_to_all(shortened(pieces[0]), "dp", split_axis=0, concat_axis=1, tiled=True),
            lax.all_to_all(shortened(pieces[1]), "dp", split_axis=0, concat_axis=1, tiled=True),
            lax.all_to_all(shortened(pieces[2]), "dp", split_axis=0, concat_axis=1, tiled=True),
            lax.all_to_all(shortened(pieces[3]), "dp", split_axis=0, concat_axis=1, tiled=True),
            lax.all_to_all(shortened(pieces[4]), "dp", split_axis=0, concat_axis=1, tiled=True),
            lax.all_to_all(shortened(pieces[5]), "dp", split_axis=0, concat_axis=1, tiled=True),
        )
        recept, key_vec, value_vec, decay_pre, rate_pre, gate_pre = [
            item.astype(jnp.float32) for item in arrived
        ]
        decay_rate = jnp.exp(-jnp.exp(-jax.nn.softplus(-(decay_base[layer_idx] + decay_pre)) - 0.5))
        learn_rate = jax.nn.sigmoid(rate_base[layer_idx] + rate_pre)
        gate_open = jax.nn.sigmoid(gate_pre)
        updated, normal_out = recur(
            state[layer_idx], recept, key_vec, value_vec, decay_rate, learn_rate, active, head_size
        )
        updated_states.append(updated)
        mixed_here = jnp.where(
            active[:, None], normal_out * group_gain[layer_idx] * gate_open, 0.0
        ).astype(jnp.bfloat16)
        rows_all = lax.all_gather(mixed_here, "dp", axis=0, tiled=True)
        out_weight = w_out[layer_idx]

        def fold_output(acc_sum, segment, offset):
            weight_rows = lax.dynamic_slice_in_dim(out_weight, offset, segment.shape[1], 0)
            return acc_sum + jnp.dot(segment, weight_rows, preferred_element_type=jnp.float32)

        blank = jnp.zeros((rows_all.shape[0], out_weight.shape[1]), jnp.float32)
        out_cols = over_axes(rows_all, TP, 1, fold_output, blank).astype(jnp.bfloat16)
        current = lax.all_to_all(out_cols, "dp", split_axis=0, concat_axis=1, tiled=True)
    return (current, jnp.stack(updated_states))


def solution(mesh):
    finer = Mesh(mesh.devices.reshape(4, 4, mesh.shape["dp"]), ("tp_0", "tp_1", "dp"))
    in_specs = (
        P("dp", TP),
        P("dp"),
        P(),
        P(None, None, TP_DP),
        P(None, None, TP_DP),
        P(None, None, TP_DP),
        P(None, None, TP_DP),
        P(None, None, TP_DP),
        P(None, None, TP_DP),
        P(None, None, TP_DP),
        P(None, TP),
        P(None, TP),
        P(None, TP),
        P(None, "dp", TP, None, None),
    )
    out_specs = (P("dp", TP), P(None, "dp", TP, None, None))
    return jax.shard_map(local, mesh=finer, in_specs=in_specs, out_specs=out_specs, check_vma=False)
```

profile of v0, /device:TPU:0, one launch (start us, length us, event | category | flops | bytes accessed | tf_op | source)
XLA Modules:
  0.0 406.6 jit_solution(4203968245207242246)
XLA Ops:
  7.3 13.6 %all_gather.36 = bf16[256,256]{1,0:T(8,128)(2,1)S(1)} all-gather(bf16[32,256]{1,0:T(8,128)(2,1)} %param.14), channel_id=1, replica_groups=mesh['tp_0'=4,'tp_1'=4,'dp'=8] {'dp'}, dimensions={0}, use_global_device_ids=true | all-gather | bytes 147456 | tf_op jit(solution)/shard_map/all_gather | solution.py:91
  20.9 14.1 %all_gather.37 = bf16[256,1024]{1,0:T(8,128)(2,1)} all-gather(bf16[256,256]{1,0:T(8,128)(2,1)S(1)} %all_gather.36), channel_id=1, replica_groups=mesh['tp_0'=4,'tp_1'=4,'dp'=8] {'tp_1'}, dimensions={1}, use_global_device_ids=true | all-gather | bytes 655360 | tf_op jit(solution)/shard_map/all_gather | solution.py:19
  43.4 24.0 %all-gather.5.cloned.1.call-done = bf16[256,4096]{1,0:T(8,128)(2,1)} async-done(((bf16[256,1024]{1,0:T(8,128)(2,1)}), bf16[256,4096]{1,0:T(8,128)(2,1)}) %all-gather.5.cloned.1.call-update) | async-done | bytes 2097168 | tf_op jit(solution)/shard_map/all_gather | solution.py:19
  67.5 2.1 fusion
  69.6 2.5 fusion.44
  72.9 4.3 %all-to-all-start = ((bf16[8,2,512]{2,1,0:T(2,128)(2,1)}), bf16[8,2,512]{2,1,0:T(2,128)(2,1)S(1)}, u32[]{:S(2)}, u32[]{:S(2)}) async-start(bf16[8,2,512]{2,1,0:T(2,128)(2,1)} %reshape.354), calls=%async_computation | async-start | bytes 32768 | tf_op jit(solution)/shard_map/all_to_all | solution.py:104
  82.6 3.9 all-to-all-start.5
  86.5 5.2 %all-to-all-done.5 = bf16[8,2,512]{2,1,0:T(2,128)(2,1)S(1)} async-done(((bf16[8,2,512]{2,1,0:T(2,128)(2,1)}), bf16[8,2,512]{2,1,0:T(2,128)(2,1)S(1)}, u32[]{:S(2)}, u32[]{:S(2)}) %all-to-all-start.5) | async-done | bytes 16416 | tf_op jit(solution)/shard_map/all_to_all | solution.py:106
  91.8 3.3 all-to-all-start.3
  95.2 5.1 %all-to-all-done.3 = bf16[8,2,512]{2,1,0:T(2,128)(2,1)S(1)} async-done(((bf16[8,2,512]{2,1,0:T(2,128)(2,1)}), bf16[8,2,512]{2,1,0:T(2,128)(2,1)S(1)}, u32[]{:S(2)}, u32[]{:S(2)}) %all-to-all-start.3) | async-done | bytes 16416 | tf_op jit(solution)/shard_map/all_to_all | solution.py:103
  100.4 3.3 all-to-all-start.1
  103.8 5.2 %all-to-all-done.1 = bf16[8,2,512]{2,1,0:T(2,128)(2,1)S(1)} async-done(((bf16[8,2,512]{2,1,0:T(2,128)(2,1)}), bf16[8,2,512]{2,1,0:T(2,128)(2,1)S(1)}, u32[]{:S(2)}, u32[]{:S(2)}) %all-to-all-start.1) | async-done | bytes 16416 | tf_op jit(solution)/shard_map/all_to_all | solution.py:102
  109.0 3.3 all-to-all-start.4
  112.4 5.2 %all-to-all-done.4 = bf16[8,2,512]{2,1,0:T(2,128)(2,1)S(1)} async-done(((bf16[8,2,512]{2,1,0:T(2,128)(2,1)}), bf16[8,2,512]{2,1,0:T(2,128)(2,1)S(1)}, u32[]{:S(2)}, u32[]{:S(2)}) %all-to-all-start.4) | async-done | bytes 16416 | tf_op jit(solution)/shard_map/all_to_all | solution.py:101
  117.6 3.3 all-to-all-start.2
  121.9 4.3 %all-to-all-done.2 = bf16[8,2,512]{2,1,0:T(2,128)(2,1)S(1)} async-done(((bf16[8,2,512]{2,1,0:T(2,128)(2,1)}), bf16[8,2,512]{2,1,0:T(2,128)(2,1)S(1)}, u32[]{:S(2)}, u32[]{:S(2)}) %all-to-all-start.2) | async-done | bytes 16416 | tf_op jit(solution)/shard_map/all_to_all | solution.py:105
  127.1 3.4 fusion.6
  130.4 4.2 %fusion.10 = f32[32,4,1,64]{3,2,1,0:T(1,128)S(1)} fusion(bf16[32,4,64,1]{2,3,1,0:T(2,128)(2,1)S(1)} %reshape.319, f32[2,32,4,64,64]{4,3,2,1,0:T(8,128)} %param.27, f32[32,4,64]{2,1,0:T(4,128)S(1)} %get-tuple-element.29, f32[32,4,64]{2,1,0:T(4,128)S(1)} %reshape.301, f32[32,4,64]{2,1,0:T(4,128)S(1)} %get-tuple-element.28, f32[32,4,64]{2,1,0:T(4,128)S(1)} %bitcast.139, ...), kind=kOutput, calls=%fused_computation.17 | convolution fusion | flops 4194304 | bytes 4407328 | tf_op jit(solution)/shard_map/bhij,bhj->bhi/dot_general | solution.py:51
  135.3 12.7 %all_gather.39 = bf16[256,256]{1,0:T(8,128)(2,1)S(1)} all-gather(bf16[32,256]{1,0:T(8,128)(2,1)S(1)} %select_convert_fusion.1), channel_id=1, replica_groups=mesh['tp_0'=4,'tp_1'=4,'dp'=8] {'dp'}, dimensions={0}, use_global_device_ids=true | all-gather | bytes 147456 | tf_op jit(solution)/shard_map/all_gather | solution.py:121
  148.1 13.9 %all_gather.40 = bf16[256,1024]{1,0:T(8,128)(2,1)} all-gather(bf16[256,256]{1,0:T(8,128)(2,1)S(1)} %all_gather.39), channel_id=1, replica_groups=mesh['tp_0'=4,'tp_1'=4,'dp'=8] {'tp_1'}, dimensions={1}, use_global_device_ids=true | all-gather | bytes 655360 | tf_op jit(solution)/shard_map/all_gather | solution.py:19
  162.1 29.0 %all-gather.7.cloned.1.call-done = bf16[256,4096]{1,0:T(8,128)(2,1)} async-done(((bf16[256,1024]{1,0:T(8,128)(2,1)}), bf16[256,4096]{1,0:T(8,128)(2,1)}) %all-gather.7.cloned.1.call-update) | async-done | bytes 2097168 | tf_op jit(solution)/shard_map/all_gather | solution.py:19
  191.1 2.3 convolution_convert_fusion.1
  193.6 9.4 %all_to_all.200 = bf16[8,2,512]{2,1,0:T(2,128)(2,1)S(1)} all-to-all(bf16[8,2,512]{2,1,0:T(2,128)(2,1)S(1)} %reshape.356), channel_id=1, replica_groups=mesh['tp_0'=4,'tp_1'=4,'dp'=8] {'dp'}, dimensions={0} | all-to-all | bytes 32768 | tf_op jit(solution)/shard_map/all_to_all | solution.py:130
  203.3 12.8 %all_gather.42 = bf16[256,256]{1,0:T(8,128)(2,1)S(1)} all-gather(bf16[32,256]{1,0:T(8,128)(2,1)S(1)} %all_to_all.168), channel_id=1, replica_groups=mesh['tp_0'=4,'tp_1'=4,'dp'=8] {'dp'}, dimensions={0}, use_global_device_ids=true | all-gather | bytes 147456 | tf_op jit(solution)/shard_map/all_gather | solution.py:91
  216.1 13.9 %all_gather.43 = bf16[256,1024]{1,0:T(8,128)(2,1)} all-gather(bf16[256,256]{1,0:T(8,128)(2,1)S(1)} %all_gather.42), channel_id=1, replica_groups=mesh['tp_0'=4,'tp_1'=4,'dp'=8] {'tp_1'}, dimensions={1}, use_global_device_ids=true | all-gather | bytes 655360 | tf_op jit(solution)/shard_map/all_gather | solution.py:19
  230.0 29.1 %all-gather.9.cloned.1.call-done = bf16[256,4096]{1,0:T(8,128)(2,1)} async-done(((bf16[256,1024]{1,0:T(8,128)(2,1)}), bf16[256,4096]{1,0:T(8,128)(2,1)}) %all-gather.9.cloned.1.call-update) | async-done | bytes 2097168 | tf_op jit(solution)/shard_map/all_gather | solution.py:19
  259.1 2.1 fusion.3
  261.2 3.0 fusion.47
  265.0 4.3 %all-to-all-start.7 = ((bf16[8,2,512]{2,1,0:T(2,128)(2,1)}), bf16[8,2,512]{2,1,0:T(2,128)(2,1)S(1)}, u32[]{:S(2)}, u32[]{:S(2)}) async-start(bf16[8,2,512]{2,1,0:T(2,128)(2,1)} %reshape.368), calls=%async_computation.7 | async-start | bytes 32768 | tf_op jit(solution)/shard_map/all_to_all | solution.py:104
  274.6 3.8 all-to-all-start.12
  278.6 5.2 %all-to-all-done.12 = bf16[8,2,512]{2,1,0:T(2,128)(2,1)S(1)} async-done(((bf16[8,2,512]{2,1,0:T(2,128)(2,1)}), bf16[8,2,512]{2,1,0:T(2,128)(2,1)S(1)}, u32[]{:S(2)}, u32[]{:S(2)}) %all-to-all-start.12) | async-done | bytes 16416 | tf_op jit(solution)/shard_map/all_to_all | solution.py:106
  283.8 3.3 all-to-all-start.10
  287.3 5.1 %all-to-all-done.10 = bf16[8,2,512]{2,1,0:T(2,128)(2,1)S(1)} async-done(((bf16[8,2,512]{2,1,0:T(2,128)(2,1)}), bf16[8,2,512]{2,1,0:T(2,128)(2,1)S(1)}, u32[]{:S(2)}, u32[]{:S(2)}) %all-to-all-start.10) | async-done | bytes 16416 | tf_op jit(solution)/shard_map/all_to_all | solution.py:103
  292.4 3.3 all-to-all-start.8
  295.9 5.2 %all-to-all-done.8 = bf16[8,2,512]{2,1,0:T(2,128)(2,1)S(1)} async-done(((bf16[8,2,512]{2,1,0:T(2,128)(2,1)}), bf16[8,2,512]{2,1,0:T(2,128)(2,1)S(1)}, u32[]{:S(2)}, u32[]{:S(2)}) %all-to-all-start.8) | async-done | bytes 16416 | tf_op jit(solution)/shard_map/all_to_all | solution.py:102
  301.0 3.3 all-to-all-start.11
  304.5 5.2 %all-to-all-done.11 = bf16[8,2,512]{2,1,0:T(2,128)(2,1)S(1)} async-done(((bf16[8,2,512]{2,1,0:T(2,128)(2,1)}), bf16[8,2,512]{2,1,0:T(2,128)(2,1)S(1)}, u32[]{:S(2)}, u32[]{:S(2)}) %all-to-all-start.11) | async-done | bytes 16416 | tf_op jit(solution)/shard_map/all_to_all | solution.py:101
  309.6 3.3 all-to-all-start.9
  313.9 4.3 %all-to-all-done.9 = bf16[8,2,512]{2,1,0:T(2,128)(2,1)S(1)} async-done(((bf16[8,2,512]{2,1,0:T(2,128)(2,1)}), bf16[8,2,512]{2,1,0:T(2,128)(2,1)S(1)}, u32[]{:S(2)}, u32[]{:S(2)}) %all-to-all-start.9) | async-done | bytes 16416 | tf_op jit(solution)/shard_map/all_to_all | solution.py:105
  319.0 3.4 fusion.11
  322.5 4.2 %fusion.15 = f32[32,4,1,64]{3,2,1,0:T(1,128)S(1)} fusion(bf16[32,4,64,1]{2,3,1,0:T(2,128)(2,1)S(1)} %reshape.321, f32[2,32,4,64,64]{4,3,2,1,0:T(8,128)} %param.27, f32[32,4,64]{2,1,0:T(4,128)S(1)} %get-tuple-element.27, f32[32,4,64]{2,1,0:T(4,128)S(1)} %reshape.307, f32[32,4,64]{2,1,0:T(4,128)S(1)} %get-tuple-element.26, f32[32,4,64]{2,1,0:T(4,128)S(1)} %bitcast.141, ...), kind=kOutput, calls=%fused_computation.24 | convolution fusion | flops 4194304 | bytes 4407328 | tf_op jit(solution)/shard_map/bhij,bhj->bhi/dot_general | solution.py:51
  327.3 12.7 %all_gather.45 = bf16[256,256]{1,0:T(8,128)(2,1)S(1)} all-gather(bf16[32,256]{1,0:T(8,128)(2,1)S(1)} %select_convert_fusion), channel_id=1, replica_groups=mesh['tp_0'=4,'tp_1'=4,'dp'=8] {'dp'}, dimensions={0}, use_global_device_ids=true | all-gather | bytes 147456 | tf_op jit(solution)/shard_map/all_gather | solution.py:121
  340.1 13.9 %all_gather.46 = bf16[256,1024]{1,0:T(8,128)(2,1)} all-gather(bf16[256,256]{1,0:T(8,128)(2,1)S(1)} %all_gather.45), channel_id=1, replica_groups=mesh['tp_0'=4,'tp_1'=4,'dp'=8] {'tp_1'}, dimensions={1}, use_global_device_ids=true | all-gather | bytes 655360 | tf_op jit(solution)/shard_map/all_gather | solution.py:19
  354.0 10.6 %add_select_fusion.1 = (f32[1,32,4,64,64]{4,3,2,1,0:T(8,128)}, f32[1,32,4,64,64]{4,3,2,1,0:T(8,128)}) fusion(f32[2,32,4,64,64]{4,3,2,1,0:T(8,128)} %param.27, f32[32,4,64]{2,1,0:T(4,128)S(1)} %get-tuple-element.29, f32[32,4,64]{2,1,0:T(4,128)S(1)} %reshape.301, f32[32,4,64]{2,1,0:T(4,128)S(1)} %get-tuple-element.28, f32[32,4,64]{2,1,0:T(4,128)S(1)} %bitcast.140, ...), kind=kLoop, calls=%fused_computation.26 | loop fusion | flops 6291456 | bytes 8716320 | tf_op jit(solution)/shard_map/jit(_where)/select_n | solution.py:50
  364.6 18.4 %all-gather.11.cloned.1.call-done = bf16[256,4096]{1,0:T(8,128)(2,1)} async-done(((bf16[256,1024]{1,0:T(8,128)(2,1)}), bf16[256,4096]{1,0:T(8,128)(2,1)}) %all-gather.11.cloned.1.call-update) | async-done | bytes 2097168 | tf_op jit(solution)/shard_map/all_gather | solution.py:19
  383.1 2.3 convolution_convert_fusion
  386.2 4.3 %all-to-all-start.13 = ((bf16[8,2,512]{2,1,0:T(2,128)(2,1)}), bf16[8,2,512]{2,1,0:T(2,128)(2,1)S(1)}, u32[]{:S(2)}, u32[]{:S(2)}) async-start(bf16[8,2,512]{2,1,0:T(2,128)(2,1)} %reshape.370), calls=%async_computation.13 | async-start | bytes 32768 | tf_op jit(solution)/shard_map/all_to_all | solution.py:130
  390.5 8.8 %pad_maximum_fusion = f32[2,32,4,64,64]{4,3,2,1,0:T(8,128)} fusion(f32[1,32,4,64,64]{4,3,2,1,0:T(8,128)} %get-tuple-element.13, f32[1,32,4,64,64]{4,3,2,1,0:T(8,128)} %get-tuple-element.12), kind=kLoop, calls=%fused_computation | loop fusion | flops 1048576 | bytes 8388608 | tf_op jit(solution)/shard_map/stack | solution.py:131
  (151 shorter events, 28.8 us)
Async XLA Ops:
  7.2 34.0 %copy-start.7 = (s32[32]{0:T(128)S(1)}, s32[32]{0:T(128)}, u32[]{:S(2)}) copy-start(s32[32]{0:T(128)} %param.15) | copy-start | bytes 388
  7.2 34.0 %copy-start.4 = (f32[2,256]{1,0:T(2,128)S(1)}, f32[2,256]{1,0:T(2,128)}, u32[]{:S(2)}) copy-start(f32[2,256]{1,0:T(2,128)} %param.26) | copy-start | bytes 6148
  7.2 34.0 %copy-start.1 = (bf16[2,4096,32]{1,2,0:T(8,128)(2,1)S(1)}, bf16[2,4096,32]{1,2,0:T(8,128)(2,1)}, u32[]{:S(2)}) copy-start(bf16[2,4096,32]{1,2,0:T(8,128)(2,1)} %param.20) | copy-start | bytes 1572868
  7.2 34.7 %copy-start.2 = (bf16[2,4096,32]{1,2,0:T(8,128)(2,1)S(1)}, bf16[2,4096,32]{1,2,0:T(8,128)(2,1)}, u32[]{:S(2)}) copy-start(bf16[2,4096,32]{1,2,0:T(8,128)(2,1)} %param.21) | copy-start | bytes 1572868
  7.2 35.5 %copy-start.3 = (bf16[2,4096,32]{1,2,0:T(8,128)(2,1)S(1)}, bf16[2,4096,32]{1,2,0:T(8,128)(2,1)}, u32[]{:S(2)}) copy-start(bf16[2,4096,32]{1,2,0:T(8,128)(2,1)} %param.22) | copy-start | bytes 1572868
  7.2 60.2 %all-gather.5.cloned.1.call-start = ((), (), s32[]{:S(2)}) async-start(), calls=%async_computation.14 | async-start | bytes 2621440 | tf_op jit(solution)/shard_map/all_gather | solution.py:19
  43.4 33.8 %copy-start.5 = (f32[2,256]{1,0:T(2,128)S(1)}, f32[2,256]{1,0:T(2,128)}, u32[]{:S(2)}) copy-start(f32[2,256]{1,0:T(2,128)} %param.25) | copy-start | bytes 6148
  43.4 33.8 %copy-start.6 = (f32[2,256]{1,0:T(2,128)S(1)}, f32[2,256]{1,0:T(2,128)}, u32[]{:S(2)}) copy-start(f32[2,256]{1,0:T(2,128)} %param.24) | copy-start | bytes 6148
  72.9 9.6 %all-to-all-start = ((bf16[8,2,512]{2,1,0:T(2,128)(2,1)}), bf16[8,2,512]{2,1,0:T(2,128)(2,1)S(1)}, u32[]{:S(2)}, u32[]{:S(2)}) async-start(bf16[8,2,512]{2,1,0:T(2,128)(2,1)} %reshape.354), calls=%async_computation | async-start | bytes 32768 | tf_op jit(solution)/shard_map/all_to_all | solution.py:104
  82.6 9.2 %all-to-all-start.5 = ((bf16[8,2,512]{2,1,0:T(2,128)(2,1)}), bf16[8,2,512]{2,1,0:T(2,128)(2,1)S(1)}, u32[]{:S(2)}, u32[]{:S(2)}) async-start(bf16[8,2,512]{2,1,0:T(2,128)(2,1)} %reshape.344), calls=%async_computation.5 | async-start | bytes 32768 | tf_op jit(solution)/shard_map/all_to_all | solution.py:106
  91.8 8.6 %all-to-all-start.3 = ((bf16[8,2,512]{2,1,0:T(2,128)(2,1)}), bf16[8,2,512]{2,1,0:T(2,128)(2,1)S(1)}, u32[]{:S(2)}, u32[]{:S(2)}) async-start(bf16[8,2,512]{2,1,0:T(2,128)(2,1)} %reshape.352), calls=%async_computation.3 | async-start | bytes 32768 | tf_op jit(solution)/shard_map/all_to_all | solution.py:103
  100.4 8.6 %all-to-all-start.1 = ((bf16[8,2,512]{2,1,0:T(2,128)(2,1)}), bf16[8,2,512]{2,1,0:T(2,128)(2,1)S(1)}, u32[]{:S(2)}, u32[]{:S(2)}) async-start(bf16[8,2,512]{2,1,0:T(2,128)(2,1)} %reshape.348), calls=%async_computation.1 | async-start | bytes 32768 | tf_op jit(solution)/shard_map/all_to_all | solution.py:102
  109.0 8.6 %all-to-all-start.4 = ((bf16[8,2,512]{2,1,0:T(2,128)(2,1)}), bf16[8,2,512]{2,1,0:T(2,128)(2,1)S(1)}, u32[]{:S(2)}, u32[]{:S(2)}) async-start(bf16[8,2,512]{2,1,0:T(2,128)(2,1)} %reshape.346), calls=%async_computation.4 | async-start | bytes 32768 | tf_op jit(solution)/shard_map/all_to_all | solution.py:101
  117.6 8.6 %all-to-all-start.2 = ((bf16[8,2,512]{2,1,0:T(2,128)(2,1)}), bf16[8,2,512]{2,1,0:T(2,128)(2,1)S(1)}, u32[]{:S(2)}, u32[]{:S(2)}) async-start(bf16[8,2,512]{2,1,0:T(2,128)(2,1)} %reshape.350), calls=%async_computation.2 | async-start | bytes 32768 | tf_op jit(solution)/shard_map/all_to_all | solution.py:105
  120.9 70.1 %all-gather.7.cloned.1.call-start = ((), (), s32[]{:S(2)}) async-start(), calls=%async_computation.15 | async-start | bytes 2621440 | tf_op jit(solution)/shard_map/all_gather | solution.py:19
  130.4 60.6 %copy-start = (bf16[2,4096,32]{1,2,0:T(8,128)(2,1)S(1)}, bf16[2,4096,32]{1,2,0:T(8,128)(2,1)}, u32[]{:S(2)}) copy-start(bf16[2,4096,32]{1,2,0:T(8,128)(2,1)} %param.23) | copy-start | bytes 1572868
  162.0 97.1 %all-gather.9.cloned.1.call-start = ((), (), s32[]{:S(2)}) async-start(), calls=%async_computation.16 | async-start | bytes 2621440 | tf_op jit(solution)/shard_map/all_gather | solution.py:19
  265.0 9.6 %all-to-all-start.7 = ((bf16[8,2,512]{2,1,0:T(2,128)(2,1)}), bf16[8,2,512]{2,1,0:T(2,128)(2,1)S(1)}, u32[]{:S(2)}, u32[]{:S(2)}) async-start(bf16[8,2,512]{2,1,0:T(2,128)(2,1)} %reshape.368), calls=%async_computation.7 | async-start | bytes 32768 | tf_op jit(solution)/shard_map/all_to_all | solution.py:104
  274.6 9.2 %all-to-all-start.12 = ((bf16[8,2,512]{2,1,0:T(2,128)(2,1)}), bf16[8,2,512]{2,1,0:T(2,128)(2,1)S(1)}, u32[]{:S(2)}, u32[]{:S(2)}) async-start(bf16[8,2,512]{2,1,0:T(2,128)(2,1)} %reshape.358), calls=%async_computation.12 | async-start | bytes 32768 | tf_op jit(solution)/shard_map/all_to_all | solution.py:106
  283.8 8.6 %all-to-all-start.10 = ((bf16[8,2,512]{2,1,0:T(2,128)(2,1)}), bf16[8,2,512]{2,1,0:T(2,128)(2,1)S(1)}, u32[]{:S(2)}, u32[]{:S(2)}) async-start(bf16[8,2,512]{2,1,0:T(2,128)(2,1)} %reshape.366), calls=%async_computation.10 | async-start | bytes 32768 | tf_op jit(solution)/shard_map/all_to_all | solution.py:103
  292.4 8.6 %all-to-all-start.8 = ((bf16[8,2,512]{2,1,0:T(2,128)(2,1)}), bf16[8,2,512]{2,1,0:T(2,128)(2,1)S(1)}, u32[]{:S(2)}, u32[]{:S(2)}) async-start(bf16[8,2,512]{2,1,0:T(2,128)(2,1)} %reshape.362), calls=%async_computation.8 | async-start | bytes 32768 | tf_op jit(solution)/shard_map/all_to_all | solution.py:102
  301.0 8.6 %all-to-all-start.11 = ((bf16[8,2,512]{2,1,0:T(2,128)(2,1)}), bf16[8,2,512]{2,1,0:T(2,128)(2,1)S(1)}, u32[]{:S(2)}, u32[]{:S(2)}) async-start(bf16[8,2,512]{2,1,0:T(2,128)(2,1)} %reshape.360), calls=%async_computation.11 | async-start | bytes 32768 | tf_op jit(solution)/shard_map/all_to_all | solution.py:101
  309.6 8.6 %all-to-all-start.9 = ((bf16[8,2,512]{2,1,0:T(2,128)(2,1)}), bf16[8,2,512]{2,1,0:T(2,128)(2,1)S(1)}, u32[]{:S(2)}, u32[]{:S(2)}) async-start(bf16[8,2,512]{2,1,0:T(2,128)(2,1)} %reshape.364), calls=%async_computation.9 | async-start | bytes 32768 | tf_op jit(solution)/shard_map/all_to_all | solution.py:105
  313.0 70.1 %all-gather.11.cloned.1.call-start = ((), (), s32[]{:S(2)}) async-start(), calls=%async_computation.17 | async-start | bytes 2621440 | tf_op jit(solution)/shard_map/all_gather | solution.py:19
  386.2 13.0 %all-to-all-start.13 = ((bf16[8,2,512]{2,1,0:T(2,128)(2,1)}), bf16[8,2,512]{2,1,0:T(2,128)(2,1)S(1)}, u32[]{:S(2)}, u32[]{:S(2)}) async-start(bf16[8,2,512]{2,1,0:T(2,128)(2,1)} %reshape.370), calls=%async_computation.13 | async-start | bytes 32768 | tf_op jit(solution)/shard_map/all_to_all | solution.py:130
Sparse Core Ops, SparseCore 0:
  35.1 32.3 all-gather.4
  162.1 28.8 all-gather.6
  230.1 28.8 all-gather.8
  354.1 28.8 all-gather.10
where the time goes:
time: 410 us; the launch traced here: 407 us
  waiting for transfers between devices  152 us (37%)
  blocking collectives  117 us (29%)
  starting transfers between devices  47.2 us (12%)
  other arithmetic  25.6 us (6%)
  matrix products  25.2 us (6%)
  local copies, waits for them, and re-layouts  24.6 us (6%)
  between operations  14.4 us (4%)
    all_gather x4, waiting for transfers between devices, gather_axes(): nearer = lax.all_gather(value, axes[-1], axis=dim, tiled=True)  101 us
    all_gather x4, blocking collectives, gather_axes(): nearer = lax.all_gather(value, axes[-1], axis=dim, tiled=True)  55.9 us
    all_gather x2, blocking collectives, local(): batch_raw = lax.all_gather(current, 'dp', axis=0, tiled=True)  26.3 us
    all_gather x2, blocking collectives, local(): rows_all = lax.all_gather(mixed_here, 'dp', axis=0, tiled=True)  25.5 us
    unnamed x50, local copies, waits for them, and re-layouts  18.4 us
    select_n x1, other arithmetic, recur(): updated = jnp.where(active[:, None, None, None], updated, state_old)  10.6 us
    all_to_all x2, waiting for transfers between devices, local(): lax.all_to_all(shortened(pieces[5]), 'dp', split_axis=0, concat_axis=1, t...  10.5 us
    all_to_all x2, waiting for transfers between devices, local(): lax.all_to_all(shortened(pieces[1]), 'dp', split_axis=0, concat_axis=1, t...  10.3 us
  transfers between devices with their start and end apart: 17, of which 16 were waited for; matrix products, arithmetic and copies ran while one was open for 10% of the time, Pallas kernels for 0%

commit v1 on v0

v1 whole, which is shorter than its diff:
```python
import math

import jax
import jax.numpy as jnp
from jax import lax
from jax.experimental import pallas as pl
from jax.experimental.pallas import tpu as pltpu
from jax.sharding import Mesh
from jax.sharding import PartitionSpec as P

STEP = 16
RMS_EPS = 1e-06
GROUP_EPS = 0.00064
MESH = pl.DeviceIdType.MESH
AXES = ("z", "y", "x")
ORDERS = ((2, 1, 0), (1, 0, 2), (0, 2, 1), (1, 2, 0))
NT = (((1,), (1,)), ((), ()))
F32 = jnp.float32
BF16 = jnp.bfloat16
DECAY_SCALE = math.exp(-0.5)


def kernel(
    tokens,
    lengths,
    norm_gain,
    w_recept,
    w_key,
    w_value,
    w_decay,
    w_rate,
    w_gate,
    w_out,
    decay_base,
    rate_base,
    group_gain,
    state,
    mixed_out,
    state_out,
    g0,
    g1,
    g2,
    g3,
    wp,
    wo,
    st,
    a2a_s,
    a2a_r,
    fin_s,
    fin_r,
    u_ref,
    w_ref,
    kl_ref,
    tok_sem,
    loc_sem,
    sib_send,
    sib_recv,
    st_sem,
    g_send,
    g_recv,
    x_send,
    x_recv,
):
    me = tuple(lax.axis_index(axis) for axis in AXES)
    core = lax.axis_index("core")
    weights = (w_recept, w_key, w_value, w_decay, w_rate, w_gate, w_out)

    def peer(dim, step):
        return lax.rem(me[dim] + step, 4)

    def device(dim, step):
        return {AXES[dim]: peer(dim, step)}

    sibling = {"core": 1 - core}

    def remote(src, dst, send, recv, where):
        return pltpu.make_async_remote_copy(
            src_ref=src, dst_ref=dst, send_sem=send, recv_sem=recv, device_id=where, device_id_type=MESH
        )

    own = pltpu.make_async_copy(tokens, g0.at[me[0], me[1], me[2]], tok_sem)
    own.start()

    def weight_dst(layer, mat):
        if mat == 6:
            return wo.at[layer, core]
        return wp.at[layer, 2 * mat + core]

    def weight_src(layer, mat):
        return weights[mat].at[layer]

    def local_weight(layer, mat):
        return pltpu.make_async_copy(
            weight_src(layer, mat), weight_dst(layer, mat), loc_sem.at[layer, mat]
        )

    def sibling_weight(layer, mat):
        return remote(
            weight_src(layer, mat),
            weight_dst(layer, mat),
            sib_send.at[layer, mat],
            sib_recv.at[layer, mat],
            sibling,
        )

    def state_in(layer):
        return pltpu.make_async_copy(state.at[layer], st.at[layer], st_sem.at[0, layer])

    def state_back(layer):
        return pltpu.make_async_copy(st.at[layer], state_out.at[layer], st_sem.at[1, layer])

    barrier = pltpu.get_barrier_semaphore()
    for dim in range(3):
        for step in range(1, 4):
            pl.semaphore_signal(barrier, inc=1, device_id=device(dim, step), device_id_type=MESH)
    pl.semaphore_signal(barrier, inc=1, device_id=sibling, device_id_type=MESH)
    for mat in range(6):
        local_weight(0, mat).start()
    pl.semaphore_wait(barrier, 10)

    def region(buf, sub, sel):
        where = tuple(pl.ds(start, size) for start, size in sel)
        if buf.shape[-1] == 256:
            tile = (pl.ds(16 * (sub // 2), 16), pl.ds(128 * (sub % 2), 128))
        else:
            tile = (pl.ds(16 * sub, 16), pl.ds(0, 128))
        return buf.at[where + tile]

    def selection(parts):
        return tuple(parts[dim] for dim in range(3))

    def send(gid, buf, sub, stage, slot, sel, dim, step):
        block = region(buf, sub, sel)
        remote(block, block, g_send.at[gid, sub, stage], g_recv.at[gid, sub, slot], device(dim, step)).start()

    def arrived(gid, buf, sub, slot, sel):
        block = region(buf, sub, sel)
        remote(block, block, g_send.at[gid, sub, 0], g_recv.at[gid, sub, slot], sibling).wait_recv()

    def own_sel(dim_sel):
        return selection([dim_sel.get(dim, (me[dim], 1)) for dim in range(3)])

    def stage_one(gid, buf):
        for step in (1, 3, 2):
            for sub, (one, two, three) in enumerate(ORDERS):
                send(gid, buf, sub, 0, step - 1, own_sel({}), one, step)

    def stage_two(gid, buf):
        for sub, (one, two, three) in enumerate(ORDERS):
            for step in range(1, 4):
                arrived(gid, buf, sub, step - 1, own_sel({one: (peer(one, 4 - step), 1)}))
            for step in (1, 3, 2):
                send(gid, buf, sub, 1, 2 + step, own_sel({one: (0, 4)}), two, step)

    def stage_three(gid, buf):
        for sub, (one, two, three) in enumerate(ORDERS):
            for step in range(1, 4):
                arrived(gid, buf, sub, 2 + step, own_sel({one: (0, 4), two: (peer(two, 4 - step), 1)}))
            low = own_sel({one: (0, 2), two: (0, 4)})
            high = own_sel({one: (2, 2), two: (0, 4)})
            send(gid, buf, sub, 2, 6, low, three, 1)
            send(gid, buf, sub, 2, 8, high, three, 3)
            send(gid, buf, sub, 2, 7, high, three, 1)
            send(gid, buf, sub, 2, 9, low, three, 3)

    def stage_four(gid, buf):
        for sub, (one, two, three) in enumerate(ORDERS):
            low = own_sel({one: (0, 2), two: (0, 4), three: (peer(three, 3), 1)})
            arrived(gid, buf, sub, 6, low)
            send(gid, buf, sub, 2, 10, low, three, 1)
            high = own_sel({one: (2, 2), two: (0, 4), three: (peer(three, 1), 1)})
            arrived(gid, buf, sub, 8, high)
            send(gid, buf, sub, 2, 11, high, three, 3)

    def stage_five(gid, buf):
        for sub, (one, two, three) in enumerate(ORDERS):
            arrived(gid, buf, sub, 7, own_sel({one: (2, 2), two: (0, 4), three: (peer(three, 3), 1)}))
            arrived(gid, buf, sub, 9, own_sel({one: (0, 2), two: (0, 4), three: (peer(three, 1), 1)}))
            arrived(gid, buf, sub, 10, own_sel({one: (0, 2), two: (0, 4), three: (peer(three, 2), 1)}))
            arrived(gid, buf, sub, 11, own_sel({one: (2, 2), two: (0, 4), three: (peer(three, 2), 1)}))

    def gather_drain(gid, buf):
        for sub, (one, two, three) in enumerate(ORDERS):
            for stage, sel in enumerate(
                ({one: (0, 3)}, {one: (0, 4), two: (0, 3)}, {one: (0, 4), two: (0, 4), three: (0, 3)})
            ):
                parts = selection([sel.get(dim, (0, 1)) for dim in range(3)])
                block = region(buf, sub, parts)
                remote(block, block, g_send.at[gid, sub, stage], g_recv.at[gid, sub, 0], sibling).wait_send()

    def exchange(eid, src, dst):
        for step in (1, 3, 2):
            remote(
                src.at[peer(2, step)],
                dst.at[me[2]],
                x_send.at[eid, step - 1],
                x_recv.at[eid, step - 1],
                device(2, step),
            ).start()

    def exchange_wait(eid, src, dst):
        for step in range(1, 4):
            slot = dst.at[peer(2, 4 - step)]
            remote(slot, slot, x_send.at[eid, step - 1], x_recv.at[eid, step - 1], sibling).wait_recv()

    def exchange_drain(eid, src, dst):
        for step in range(1, 4):
            slot = src.at[peer(2, step)]
            remote(slot, slot, x_send.at[eid, step - 1], x_recv.at[eid, step - 1], sibling).wait_send()

    def weights_ready(layer, mats):
        for mat in mats:
            local_weight(layer, mat).wait()
            remote(
                weight_src(layer, mat),
                other_dst(layer, mat),
                sib_send.at[layer, mat],
                sib_recv.at[layer, mat],
                sibling,
            ).wait_recv()

    def other_dst(layer, mat):
        if mat == 6:
            return wo.at[layer, 1 - core]
        return wp.at[layer, 2 * mat + 1 - core]

    def scale_weights(layer):
        def body(idx, carry):
            for part in range(4):
                cols = slice(1024 * part, 1024 * (part + 1))
                gain = norm_gain[layer : layer + 1, cols]
                wp[layer, idx, :, cols] = (wp[layer, idx, :, cols].astype(F32) * gain).astype(BF16)
            return carry

        lax.fori_loop(0, 12, body, 0)

    ones = jnp.ones((8, 256), BF16)

    def project(layer, buf):
        acc = jnp.zeros((384, 128), F32)
        squares = jnp.zeros((8, 128), F32)
        for group in range(16):
            weight = wp[layer, :, :, 256 * group : 256 * (group + 1)].reshape(384, 256)
            if layer == 0:
                block = buf[group // 4, group % 4].reshape(128, 256)
                acc += lax.dot_general(weight, block, NT, preferred_element_type=F32)
                squares += lax.dot_general(ones, block * block, NT, preferred_element_type=F32)
            else:
                block = buf[group // 4, group % 4].reshape(256, 128)
                acc += jnp.dot(weight, block, preferred_element_type=F32)
                squares += jnp.dot(ones, block * block, preferred_element_type=F32)
        factor = lax.rsqrt(squares[0:1, :] * (1.0 / 4096) + RMS_EPS)
        rows = jnp.transpose(acc * factor).astype(BF16)
        a2a_s[layer] = rows.reshape(4, 32, 384)

    def head_parts(row):
        return [row[:, 64 * head : 64 * (head + 1)] for head in range(4)]

    lane_len = lengths[...].astype(F32)
    diag = lax.broadcasted_iota(jnp.int32, (32, 32), 0) == lax.broadcasted_iota(jnp.int32, (32, 32), 1)
    active = jnp.sum(jnp.where(diag, lane_len, 0.0), axis=1, keepdims=True) > STEP
    row_of = lax.broadcasted_iota(jnp.int32, (8, 64), 0)

    def recur(layer):
        decay_parts = head_parts(decay_base[layer : layer + 1, :])
        rate_parts = head_parts(rate_base[layer : layer + 1, :])
        gain_parts = head_parts(group_gain[layer : layer + 1, :])
        results = []
        for head in range(4):
            tile = a2a_r[layer, head].astype(F32)
            recept, key, value, decay, rate, gate = [
                tile[:, 64 * mat : 64 * (mat + 1)] for mat in range(6)
            ]
            size = jnp.maximum(jnp.sqrt(jnp.sum(key * key, axis=1, keepdims=True)), 1e-12)
            unit = key / size
            keep = jnp.exp(-DECAY_SCALE * jax.nn.sigmoid(decay_parts[head] + decay))
            unit_rate = unit * jax.nn.sigmoid(rate_parts[head] + rate)
            beta = jnp.sum(unit_rate * recept, axis=1, keepdims=True)
            probe = (keep * recept).astype(BF16)
            unit_b = unit.astype(BF16)
            along, read = [], []
            for octet in range(4):
                rows = slice(8 * octet, 8 * octet + 8)
                left = jnp.concatenate([unit_b[rows], probe[rows]], axis=0)
                sum_a = jnp.zeros((8, 64), F32)
                sum_r = jnp.zeros((8, 64), F32)
                for low in range(8):
                    seq = 8 * octet + low
                    matrix = st[layer, seq, head].astype(BF16)
                    both = lax.dot_general(left, matrix, NT, preferred_element_type=F32)
                    sum_a = jnp.where(row_of == low, both[0:8], sum_a)
                    sum_r = jnp.where(row_of == low, both[8:16], sum_r)
                along.append(sum_a)
                read.append(sum_r)
            delta = size * value - jnp.concatenate(along, axis=0)
            readout = jnp.concatenate(read, axis=0) + delta * beta
            centre = jnp.mean(readout, axis=1, keepdims=True)
            moved = readout - centre
            spread = jnp.mean(moved * moved, axis=1, keepdims=True)
            normal = moved * lax.rsqrt(spread + GROUP_EPS) * gain_parts[head]
            results.append(jnp.where(active, normal * jax.nn.sigmoid(gate), 0.0))
            u_ref[head] = jnp.transpose(delta)
            w_ref[head] = jnp.where(active, keep, 1.0)
            kl_ref[head] = jnp.where(active, unit_rate, 0.0)
        return jnp.concatenate(results, axis=1).astype(BF16)

    def update_state(layer):
        for head in range(4):
            column = u_ref[head]
            for seq in range(32):
                st[layer, seq, head] = (
                    st[layer, seq, head] * w_ref[head, seq : seq + 1, :]
                    + column[:, seq : seq + 1] * kl_ref[head, seq : seq + 1, :]
                )

    def output(layer, buf):
        acc = jnp.zeros((64, 128), F32)
        for group in range(16):
            weight = wo[layer, :, :, 256 * group : 256 * (group + 1)].reshape(64, 256)
            block = buf[group // 4, group % 4].reshape(128, 256)
            acc += lax.dot_general(weight, block, NT, preferred_element_type=F32)
        return acc

    def store_own(buf, value):
        buf[me[0], me[1], me[2]] = value

    own.wait()
    stage_one(0, g0)
    for mat in range(6):
        sibling_weight(0, mat).start()
    state_in(0).start()
    local_weight(0, 6).start()
    sibling_weight(0, 6).start()
    stage_two(0, g0)
    stage_three(0, g0)
    for mat in range(7):
        local_weight(1, mat).start()
        sibling_weight(1, mat).start()
    state_in(1).start()
    weights_ready(0, range(6))
    stage_four(0, g0)
    scale_weights(0)
    stage_five(0, g0)
    project(0, g0)
    exchange(0, a2a_s.at[0], a2a_r.at[0])
    a2a_r[0, me[2]] = a2a_s[0, me[2]]
    state_in(0).wait()
    exchange_wait(0, a2a_s.at[0], a2a_r.at[0])
    store_own(g1, recur(0))
    stage_one(1, g1)
    weights_ready(0, (6,))
    stage_two(1, g1)
    stage_three(1, g1)
    stage_four(1, g1)
    update_state(0)
    state_back(0).start()
    stage_five(1, g1)
    store_own(g2, output(0, g1).astype(BF16))
    stage_one(2, g2)
    weights_ready(1, range(7))
    stage_two(2, g2)
    stage_three(2, g2)
    stage_four(2, g2)
    scale_weights(1)
    stage_five(2, g2)
    project(1, g2)
    exchange(1, a2a_s.at[1], a2a_r.at[1])
    a2a_r[1, me[2]] = a2a_s[1, me[2]]
    state_in(1).wait()
    exchange_wait(1, a2a_s.at[1], a2a_r.at[1])
    store_own(g3, recur(1))
    stage_one(3, g3)
    stage_two(3, g3)
    stage_three(3, g3)
    stage_four(3, g3)
    update_state(1)
    state_back(1).start()
    stage_five(3, g3)
    fin_s[...] = jnp.transpose(output(1, g3)).astype(BF16).reshape(4, 32, 64)
    exchange(2, fin_s, fin_r)
    fin_r[me[2]] = fin_s[me[2]]
    exchange_wait(2, fin_s, fin_r)
    mixed_out[...] = jnp.concatenate([fin_r[head].astype(F32) for head in range(4)], axis=1).astype(BF16)
    for layer in range(2):
        for mat in range(7):
            sibling_weight(layer, mat).wait_send()
    for gid, buf in enumerate((g0, g1, g2, g3)):
        gather_drain(gid, buf)
    exchange_drain(0, a2a_s.at[0], a2a_r.at[0])
    exchange_drain(1, a2a_s.at[1], a2a_r.at[1])
    exchange_drain(2, fin_s, fin_r)
    state_back(0).wait()
    state_back(1).wait()


def local(tokens, lengths, norm_gain, *rest):
    weights = [jnp.swapaxes(weight, 1, 2) for weight in rest[:7]]
    decay_base, rate_base, group_gain, state = rest[7:]
    vmem = pl.BlockSpec(memory_space=pltpu.VMEM)
    anywhere = pl.BlockSpec(memory_space=pl.ANY)
    rows_block = pltpu.VMEM((4, 4, 4, 32, 256), BF16)
    dma = pltpu.SemaphoreType.DMA
    return pl.pallas_call(
        kernel,
        out_shape=(
            jax.ShapeDtypeStruct((32, 256), BF16),
            jax.ShapeDtypeStruct(state.shape, F32),
        ),
        in_specs=[anywhere, vmem, vmem] + [anywhere] * 7 + [vmem] * 3 + [anywhere],
        out_specs=(vmem, anywhere),
        scratch_shapes=[
            rows_block,
            rows_block,
            pltpu.VMEM((4, 4, 4, 64, 128), BF16),
            rows_block,
            pltpu.VMEM((2, 12, 32, 4096), BF16),
            pltpu.VMEM((2, 2, 32, 4096), BF16),
            pltpu.VMEM((2, 32, 4, 64, 64), F32),
            pltpu.VMEM((2, 4, 32, 384), BF16),
            pltpu.VMEM((2, 4, 32, 384), BF16),
            pltpu.VMEM((4, 32, 64), BF16),
            pltpu.VMEM((4, 32, 64), BF16),
            pltpu.VMEM((4, 64, 32), F32),
            pltpu.VMEM((4, 32, 64), F32),
            pltpu.VMEM((4, 32, 64), F32),
            dma,
            dma((2, 7)),
            dma((2, 7)),
            dma((2, 7)),
            dma((2, 2)),
            dma((4, 4, 3)),
            dma((4, 4, 12)),
            dma((3, 3)),
            dma((3, 3)),
        ],
        compiler_params=pltpu.CompilerParams(
            collective_id=0, has_side_effects=True, vmem_limit_bytes=60 * 1024 * 1024
        ),
    )(tokens, lengths.reshape(1, 32), norm_gain, *weights, decay_base, rate_base, group_gain, state)


def solution(mesh):
    finer = Mesh(mesh.devices.reshape(4, 4, 4, 2), ("z", "y", "x", "core"))
    tp, dp = ("z", "y"), ("x", "core")
    weight = P(None, None, tp + dp)
    vector = P(None, tp)
    states = P(None, dp, tp, None, None)
    in_specs = (P(dp, tp), P(dp), P()) + (weight,) * 7 + (vector,) * 3 + (states,)
    return jax.shard_map(
        local, mesh=finer, in_specs=in_specs, out_specs=(P(dp, tp), states), check_vma=False
    )
```

time: 410 us -> 103 us (0.25)
  waiting for transfers between devices: 152 us -> 0 us
  blocking collectives: 117 us -> 0 us
  Pallas kernels: 0 us -> 92.1 us
  starting transfers between devices: 47.2 us -> 0 us
  other arithmetic: 25.6 us -> 0 us
  matrix products: 25.2 us -> 0 us
  local copies, waits for them, and re-layouts: 24.6 us -> 9.76 us
  between operations: 14.4 us -> 0.64 us
    all_gather x8 -> x0, blocking collectives: 108 us -> none  [the longest x4 55.9 us: gather_axes(): nearer = lax.all_gather(value, axes[-1], axis=dim, tiled=True)]
    all_gather x4 -> x0, waiting for transfers between devices: 101 us -> none  [gather_axes(): nearer = lax.all_gather(value, axes[-1], axis=dim, tiled=True)]
    pallas_call x0 -> x1, Pallas kernels: none -> 92.1 us  [local(): pl.pallas_call(kernel, out_shape=(jax.ShapeDtypeStruct((32, 256), BF16),...]
    all_to_all x13 -> x0, waiting for transfers between devices: 51.9 us -> none  [the longest x2 10.5 us: local(): lax.all_to_all(shortened(pieces[5]), 'dp', split_axis=0, concat_axis=1, t...]
    all_to_all x13 -> x0, starting transfers between devices: 47 us -> none  [the longest x2 8.51 us: local(): lax.all_to_all(shortened(pieces[3]), 'dp', split_axis=0, concat_axis=1, t...]
    dot_general x8 -> x0, matrix products: 25.2 us -> none  [the longest x2 8.39 us: recur(): jnp.einsum('bhij,bhj->bhi', updated, recept_h, precision=lax.Precision.DE...]
    select_n x1 -> x0, other arithmetic: 10.6 us -> none  [recur(): updated = jnp.where(active[:, None, None, None], updated, state_old)]
    all_to_all x1 -> x0, blocking collectives: 9.41 us -> none  [local(): lax.all_to_all(out_cols, 'dp', split_axis=0, concat_axis=1, tiled=True)]
  transfers between devices with their start and end apart: 17 -> 0, of which waited for: 16 -> 0; matrix products, arithmetic and copies ran while one was open for 10% -> 0% of each run, Pallas kernels for 0% -> 0%
where the time goes in v1:
time: 103 us
  Pallas kernels  92.1 us (89%)
  local copies, waits for them, and re-layouts  9.76 us (9%)
    pallas_call x1, Pallas kernels, local(): pl.pallas_call(kernel, out_shape=(jax.ShapeDtypeStruct((32, 256), BF16),...  92.1 us
    unnamed x2, local copies, waits for them, and re-layouts  9.76 us

profile of v1, /device:TPU:0, one launch (start us, length us, event | category | flops | bytes accessed | tf_op | source)
XLA Modules:
  0.0 102.5 jit_solution(5093362587589882465)
XLA Ops:
  0.6 92.1 %shard_map.149 = (bf16[32,256]{1,0:T(8,128)(2,1)}, f32[2,32,4,64,64]{4,3,2,1,0:T(8,128)}) custom-call(bf16[32,256]{1,0:T(8,128)(2,1)} %tokens.1, s32[1,32]{1,0:T(1,128)} %bitcast.15, f32[2,4096]{1,0:T(2,128)} %norm_gain.1, bf16[2,32,4096]{2,1,0:T(8,128)(2,1)} %bitcast.8, bf16[2,32,4096]{2,1,0:T(8,128)(2,1)} %bitcast.9, bf16[2,32,4096]{2,1,0:T(8,128)(2,1)} %bitcast.10, ...), custom_call_target="tpu_custom_call" | custom-call | tf_op jit(solution)/shard_map/pallas_call | solution.py:403
  92.8 1.3 %copy.18 = bf16[32,256]{1,0:T(8,128)(2,1)} copy(bf16[32,256]{1,0:T(8,128)(2,1)} %get-tuple-element.4) | data formatting | bytes 32768
  94.1 8.4 %copy.19 = f32[2,32,4,64,64]{4,3,2,1,0:T(8,128)} copy(f32[2,32,4,64,64]{4,3,2,1,0:T(8,128)} %get-tuple-element.5) | data formatting | bytes 8388608

commit v2 on v1

--- a/solution.py
+++ b/solution.py
@@ -14,6 +14,10 @@
 MESH = pl.DeviceIdType.MESH
 AXES = ("z", "y", "x")
 ORDERS = ((2, 1, 0), (1, 0, 2), (0, 2, 1), (1, 2, 0))
+PLANE = sorted(
+    [(dz, dy) for dz in range(4) for dy in range(4) if dz or dy],
+    key=lambda offset: -min(offset[0], 4 - offset[0]) - min(offset[1], 4 - offset[1]),
+)
 NT = (((1,), (1,)), ((), ()))
 F32 = jnp.float32
 BF16 = jnp.bfloat16
@@ -22,8 +26,8 @@
 
 def kernel(
     tokens,
-    lengths,
-    norm_gain,
+    lengths_hbm,
+    norm_gain_hbm,
     w_recept,
     w_key,
     w_value,
@@ -31,33 +35,42 @@
     w_rate,
     w_gate,
     w_out,
-    decay_base,
-    rate_base,
-    group_gain,
+    decay_base_hbm,
+    rate_base_hbm,
+    group_gain_hbm,
     state,
     mixed_out,
-    state_out,
+    st,
     g0,
     g1,
     g2,
     g3,
     wp,
     wo,
-    st,
     a2a_s,
     a2a_r,
-    fin_s,
-    fin_r,
     u_ref,
     w_ref,
     kl_ref,
+    lengths,
+    norm_gain,
+    decay_base,
+    rate_base,
+    group_gain,
     tok_sem,
+    small_sem,
     loc_sem,
     sib_send,
     sib_recv,
     st_sem,
     g_send,
     g_recv,
+    p_send,
+    p_recv,
+    r_send,
+    r_recv,
+    d_send,
+    d_recv,
     x_send,
     x_recv,
 ):
@@ -71,6 +84,9 @@
     def device(dim, step):
         return {AXES[dim]: peer(dim, step)}
 
+    def plane_device(dz, dy):
+        return {"z": peer(0, dz), "y": peer(1, dy)}
+
     sibling = {"core": 1 - core}
 
     def remote(src, dst, send, recv, where):
@@ -83,7 +99,7 @@
 
     def weight_dst(layer, mat):
         if mat == 6:
-            return wo.at[layer, core]
+            return wo.at[layer, me[2], core]
         return wp.at[layer, 2 * mat + core]
 
     def weight_src(layer, mat):
@@ -104,26 +120,33 @@
         )
 
     def state_in(layer):
-        return pltpu.make_async_copy(state.at[layer], st.at[layer], st_sem.at[0, layer])
-
-    def state_back(layer):
-        return pltpu.make_async_copy(st.at[layer], state_out.at[layer], st_sem.at[1, layer])
+        return pltpu.make_async_copy(state.at[layer], st.at[layer], st_sem.at[layer])
 
     barrier = pltpu.get_barrier_semaphore()
-    for dim in range(3):
-        for step in range(1, 4):
-            pl.semaphore_signal(barrier, inc=1, device_id=device(dim, step), device_id_type=MESH)
-    pl.semaphore_signal(barrier, inc=1, device_id=sibling, device_id_type=MESH)
+    partners = [device(2, step) for step in range(1, 4)] + [plane_device(*offset) for offset in PLANE] + [sibling]
+    for partner in partners:
+        pl.semaphore_signal(barrier, inc=1, device_id=partner, device_id_type=MESH)
     for mat in range(6):
         local_weight(0, mat).start()
-    pl.semaphore_wait(barrier, 10)
+    small = [
+        pltpu.make_async_copy(src, dst, small_sem.at[idx])
+        for idx, (src, dst) in enumerate(
+            (
+                (norm_gain_hbm, norm_gain),
+                (lengths_hbm, lengths),
+                (decay_base_hbm, decay_base),
+                (rate_base_hbm, rate_base),
+                (group_gain_hbm, group_gain),
+            )
+        )
+    ]
+    for copy in small:
+        copy.start()
+    pl.semaphore_wait(barrier, len(partners))
 
     def region(buf, sub, sel):
         where = tuple(pl.ds(start, size) for start, size in sel)
-        if buf.shape[-1] == 256:
-            tile = (pl.ds(16 * (sub // 2), 16), pl.ds(128 * (sub % 2), 128))
-        else:
-            tile = (pl.ds(16 * sub, 16), pl.ds(0, 128))
+        tile = (pl.ds(16 * (sub // 2), 16), pl.ds(128 * (sub % 2), 128))
         return buf.at[where + tile]
 
     def selection(parts):
@@ -188,6 +211,75 @@
                 block = region(buf, sub, parts)
                 remote(block, block, g_send.at[gid, sub, stage], g_recv.at[gid, sub, 0], sibling).wait_send()
 
+    def plane_start(pid, buf):
+        block = buf.at[me[0], me[1]]
+        for dz, dy in PLANE:
+            remote(
+                block, block, p_send.at[pid, min(dz, 1)], p_recv.at[pid, 4 * dz + dy - 1], plane_device(dz, dy)
+            ).start()
+
+    def plane_wait(pid, buf):
+        for dz, dy in PLANE[::-1]:
+            block = buf.at[peer(0, 4 - dz), peer(1, 4 - dy)]
+            remote(block, block, p_send.at[pid, 0], p_recv.at[pid, 4 * dz + dy - 1], sibling).wait_recv()
+
+    def plane_drain(pid, buf):
+        for idx, block in enumerate((buf.at[pl.ds(0, 1), pl.ds(0, 3)], buf.at[pl.ds(0, 3)])):
+            remote(block, block, p_send.at[pid, idx], p_recv.at[pid, 0], sibling).wait_send()
+
+    def half(ref, part):
+        return ref.at[pl.ds(16 * part, 16)]
+
+    def ring_start(layer):
+        for step, part, slot in ((1, 0, 0), (3, 1, 2), (1, 1, 1), (3, 0, 3)):
+            remote(
+                half(w_out.at[layer], part),
+                half(wo.at[layer, me[2], core], part),
+                r_send.at[layer, slot],
+                r_recv.at[layer, slot],
+                device(2, step),
+            ).start()
+
+    RING = ((3, 0), (3, 1), (1, 1), (1, 0), (2, 0), (2, 1))
+
+    def ring_wait(layer, slot):
+        step, part = RING[slot]
+        piece = half(wo.at[layer, peer(2, step), core], part)
+        remote(piece, piece, r_send.at[layer, slot], r_recv.at[layer, slot], sibling).wait_recv()
+
+    def ring_pass(layer):
+        for slot, onward, step in ((0, 4, 1), (2, 5, 3)):
+            ring_wait(layer, slot)
+            source, part = RING[slot]
+            piece = half(wo.at[layer, peer(2, source), core], part)
+            remote(piece, piece, r_send.at[layer, onward], r_recv.at[layer, onward], device(2, step)).start()
+
+    def across(layer, step, which):
+        piece = wo.at[layer, peer(2, step), which]
+        return remote(piece, piece, d_send.at[layer, step - 1], d_recv.at[layer, step - 1], sibling)
+
+    def ring_near(layer):
+        ring_wait(layer, 1)
+        across(layer, 3, core).start()
+        ring_wait(layer, 3)
+        across(layer, 1, core).start()
+
+    def ring_far(layer):
+        ring_wait(layer, 4)
+        ring_wait(layer, 5)
+        across(layer, 2, core).start()
+
+    def ring_done(layer):
+        for step in (3, 1, 2):
+            across(layer, step, 1 - core).wait_recv()
+
+    def ring_drain(layer):
+        for step in (3, 1, 2):
+            across(layer, step, core).wait_send()
+        for slot in range(6):
+            piece = half(wo.at[layer, 0, 0], 0)
+            remote(piece, piece, r_send.at[layer, slot], r_recv.at[layer, slot], sibling).wait_send()
+
     def exchange(eid, src, dst):
         for step in (1, 3, 2):
             remote(
@@ -221,7 +313,7 @@
 
     def other_dst(layer, mat):
         if mat == 6:
-            return wo.at[layer, 1 - core]
+            return wo.at[layer, me[2], 1 - core]
         return wp.at[layer, 2 * mat + 1 - core]
 
     def scale_weights(layer):
@@ -241,14 +333,9 @@
         squares = jnp.zeros((8, 128), F32)
         for group in range(16):
             weight = wp[layer, :, :, 256 * group : 256 * (group + 1)].reshape(384, 256)
-            if layer == 0:
-                block = buf[group // 4, group % 4].reshape(128, 256)
-                acc += lax.dot_general(weight, block, NT, preferred_element_type=F32)
-                squares += lax.dot_general(ones, block * block, NT, preferred_element_type=F32)
-            else:
-                block = buf[group // 4, group % 4].reshape(256, 128)
-                acc += jnp.dot(weight, block, preferred_element_type=F32)
-                squares += jnp.dot(ones, block * block, preferred_element_type=F32)
+            block = buf[group // 4, group % 4].reshape(128, 256)
+            acc += lax.dot_general(weight, block, NT, preferred_element_type=F32)
+            squares += lax.dot_general(ones, block * block, NT, preferred_element_type=F32)
         factor = lax.rsqrt(squares[0:1, :] * (1.0 / 4096) + RMS_EPS)
         rows = jnp.transpose(acc * factor).astype(BF16)
         a2a_s[layer] = rows.reshape(4, 32, 384)
@@ -256,12 +343,12 @@
     def head_parts(row):
         return [row[:, 64 * head : 64 * (head + 1)] for head in range(4)]
 
-    lane_len = lengths[...].astype(F32)
-    diag = lax.broadcasted_iota(jnp.int32, (32, 32), 0) == lax.broadcasted_iota(jnp.int32, (32, 32), 1)
-    active = jnp.sum(jnp.where(diag, lane_len, 0.0), axis=1, keepdims=True) > STEP
     row_of = lax.broadcasted_iota(jnp.int32, (8, 64), 0)
 
     def recur(layer):
+        lane_len = lengths[...].astype(F32)
+        diag = lax.broadcasted_iota(jnp.int32, (32, 32), 0) == lax.broadcasted_iota(jnp.int32, (32, 32), 1)
+        active = jnp.sum(jnp.where(diag, lane_len, 0.0), axis=1, keepdims=True) > STEP
         decay_parts = head_parts(decay_base[layer : layer + 1, :])
         rate_parts = head_parts(rate_base[layer : layer + 1, :])
         gain_parts = head_parts(group_gain[layer : layer + 1, :])
@@ -314,129 +401,168 @@
                 )
 
     def output(layer, buf):
-        acc = jnp.zeros((64, 128), F32)
+        acc = jnp.zeros((256, 32), F32)
         for group in range(16):
-            weight = wo[layer, :, :, 256 * group : 256 * (group + 1)].reshape(64, 256)
-            block = buf[group // 4, group % 4].reshape(128, 256)
-            acc += lax.dot_general(weight, block, NT, preferred_element_type=F32)
-        return acc
-
-    def store_own(buf, value):
-        buf[me[0], me[1], me[2]] = value
-
-    own.wait()
-    stage_one(0, g0)
-    for mat in range(6):
-        sibling_weight(0, mat).start()
-    state_in(0).start()
-    local_weight(0, 6).start()
-    sibling_weight(0, 6).start()
-    stage_two(0, g0)
-    stage_three(0, g0)
-    for mat in range(7):
-        local_weight(1, mat).start()
-        sibling_weight(1, mat).start()
-    state_in(1).start()
-    weights_ready(0, range(6))
-    stage_four(0, g0)
-    scale_weights(0)
-    stage_five(0, g0)
-    project(0, g0)
-    exchange(0, a2a_s.at[0], a2a_r.at[0])
-    a2a_r[0, me[2]] = a2a_s[0, me[2]]
-    state_in(0).wait()
-    exchange_wait(0, a2a_s.at[0], a2a_r.at[0])
-    store_own(g1, recur(0))
-    stage_one(1, g1)
-    weights_ready(0, (6,))
-    stage_two(1, g1)
-    stage_three(1, g1)
-    stage_four(1, g1)
-    update_state(0)
-    state_back(0).start()
-    stage_five(1, g1)
-    store_own(g2, output(0, g1).astype(BF16))
-    stage_one(2, g2)
-    weights_ready(1, range(7))
-    stage_two(2, g2)
-    stage_three(2, g2)
-    stage_four(2, g2)
-    scale_weights(1)
-    stage_five(2, g2)
-    project(1, g2)
-    exchange(1, a2a_s.at[1], a2a_r.at[1])
-    a2a_r[1, me[2]] = a2a_s[1, me[2]]
-    state_in(1).wait()
-    exchange_wait(1, a2a_s.at[1], a2a_r.at[1])
-    store_own(g3, recur(1))
-    stage_one(3, g3)
-    stage_two(3, g3)
-    stage_three(3, g3)
-    stage_four(3, g3)
-    update_state(1)
-    state_back(1).start()
-    stage_five(3, g3)
-    fin_s[...] = jnp.transpose(output(1, g3)).astype(BF16).reshape(4, 32, 64)
-    exchange(2, fin_s, fin_r)
-    fin_r[me[2]] = fin_s[me[2]]
-    exchange_wait(2, fin_s, fin_r)
-    mixed_out[...] = jnp.concatenate([fin_r[head].astype(F32) for head in range(4)], axis=1).astype(BF16)
-    for layer in range(2):
+            weight = wo[layer, :, :, :, 256 * group : 256 * (group + 1)].reshape(256, 256)
+            acc += lax.dot_general(weight, buf[group // 4, group % 4], NT, preferred_element_type=F32)
+        return jnp.transpose(acc).astype(BF16)
+
+    def start_weights(layer, mats):
+        for mat in mats:
+            local_weight(layer, mat).start()
+            sibling_weight(layer, mat).start()
+
+    def drain_weights(layer):
         for mat in range(7):
             sibling_weight(layer, mat).wait_send()
-    for gid, buf in enumerate((g0, g1, g2, g3)):
-        gather_drain(gid, buf)
-    exchange_drain(0, a2a_s.at[0], a2a_r.at[0])
-    exchange_drain(1, a2a_s.at[1], a2a_r.at[1])
-    exchange_drain(2, fin_s, fin_r)
-    state_back(0).wait()
-    state_back(1).wait()
+
+    scope = jax.named_scope
+    with scope("g0_one"):
+        own.wait()
+        stage_one(0, g0)
+        for mat in range(6):
+            sibling_weight(0, mat).start()
+        state_in(0).start()
+        start_weights(0, (6,))
+    buffers = ((g0, g1), (g2, g3))
+    for layer in range(2):
+        wide, rows = buffers[layer]
+        with scope("two"):
+            stage_two(layer, wide)
+        with scope("three"):
+            stage_three(layer, wide)
+            if layer == 0:
+                for copy in small:
+                    copy.wait()
+                start_weights(1, range(7))
+                state_in(1).start()
+        with scope("four"):
+            stage_four(layer, wide)
+        with scope("scale"):
+            weights_ready(layer, range(7))
+            scale_weights(layer)
+            drain_weights(layer)
+        with scope("five"):
+            stage_five(layer, wide)
+        with scope("project"):
+            project(layer, wide)
+        with scope("exchange"):
+            exchange(layer, a2a_s.at[layer], a2a_r.at[layer])
+            a2a_r[layer, me[2]] = a2a_s[layer, me[2]]
+            gather_drain(layer, wide)
+            state_in(layer).wait()
+            exchange_wait(layer, a2a_s.at[layer], a2a_r.at[layer])
+            ring_start(layer)
+        with scope("recur"):
+            rows[me[0], me[1]] = recur(layer)
+        with scope("plane"):
+            plane_start(layer, rows)
+        with scope("update"):
+            update_state(layer)
+        with scope("ring"):
+            ring_pass(layer)
+            exchange_drain(layer, a2a_s.at[layer], a2a_r.at[layer])
+            ring_near(layer)
+        with scope("far"):
+            ring_far(layer)
+        with scope("plane_wait"):
+            plane_wait(layer, rows)
+        with scope("ring_done"):
+            ring_done(layer)
+        with scope("output"):
+            result = output(layer, rows)
+            if layer == 0:
+                g2[me[0], me[1], me[2]] = result
+            else:
+                mixed_out[...] = result
+        with scope("drain"):
+            if layer == 0:
+                stage_one(1, g2)
+            plane_drain(layer, rows)
+            ring_drain(layer)
+
+
+def flush(mixed, updated, mixed_out, state_out, sems):
+    copies = [
+        pltpu.make_async_copy(
+            updated.at[layer, pl.ds(8 * part, 8)], state_out.at[layer, pl.ds(8 * part, 8)], sems.at[layer, part]
+        )
+        for layer in range(2)
+        for part in range(4)
+    ]
+    for copy in copies:
+        copy.start()
+    mixed_out[...] = mixed[...]
+    for copy in copies:
+        copy.wait()
 
 
 def local(tokens, lengths, norm_gain, *rest):
     weights = [jnp.swapaxes(weight, 1, 2) for weight in rest[:7]]
     decay_base, rate_base, group_gain, state = rest[7:]
+    operands = [tokens, lengths.reshape(1, 32), norm_gain, *weights, decay_base, rate_base, group_gain, state]
+    operands = [pltpu.with_memory_space_constraint(operand, pltpu.HBM) for operand in operands]
     vmem = pl.BlockSpec(memory_space=pltpu.VMEM)
-    anywhere = pl.BlockSpec(memory_space=pl.ANY)
-    rows_block = pltpu.VMEM((4, 4, 4, 32, 256), BF16)
+    anywhere = pl.BlockSpec(memory_space=pltpu.HBM)
     dma = pltpu.SemaphoreType.DMA
-    return pl.pallas_call(
+    mixed, updated = pl.pallas_call(
         kernel,
         out_shape=(
             jax.ShapeDtypeStruct((32, 256), BF16),
             jax.ShapeDtypeStruct(state.shape, F32),
         ),
-        in_specs=[anywhere, vmem, vmem] + [anywhere] * 7 + [vmem] * 3 + [anywhere],
-        out_specs=(vmem, anywhere),
+        in_specs=[anywhere] * 14,
+        out_specs=(vmem, vmem),
         scratch_shapes=[
-            rows_block,
-            rows_block,
-            pltpu.VMEM((4, 4, 4, 64, 128), BF16),
-            rows_block,
+            pltpu.VMEM((4, 4, 4, 32, 256), BF16),
+            pltpu.VMEM((4, 4, 32, 256), BF16),
+            pltpu.VMEM((4, 4, 4, 32, 256), BF16),
+            pltpu.VMEM((4, 4, 32, 256), BF16),
             pltpu.VMEM((2, 12, 32, 4096), BF16),
-            pltpu.VMEM((2, 2, 32, 4096), BF16),
-            pltpu.VMEM((2, 32, 4, 64, 64), F32),
+            pltpu.VMEM((2, 4, 2, 32, 4096), BF16),
             pltpu.VMEM((2, 4, 32, 384), BF16),
             pltpu.VMEM((2, 4, 32, 384), BF16),
-            pltpu.VMEM((4, 32, 64), BF16),
-            pltpu.VMEM((4, 32, 64), BF16),
             pltpu.VMEM((4, 64, 32), F32),
             pltpu.VMEM((4, 32, 64), F32),
             pltpu.VMEM((4, 32, 64), F32),
+            pltpu.VMEM((1, 32), jnp.int32),
+            pltpu.VMEM((2, 4096), F32),
+            pltpu.VMEM((2, 256), F32),
+            pltpu.VMEM((2, 256), F32),
+            pltpu.VMEM((2, 256), F32),
             dma,
+            dma((5,)),
             dma((2, 7)),
             dma((2, 7)),
             dma((2, 7)),
+            dma((2,)),
+            dma((2, 4, 3)),
+            dma((2, 4, 12)),
             dma((2, 2)),
-            dma((4, 4, 3)),
-            dma((4, 4, 12)),
-            dma((3, 3)),
-            dma((3, 3)),
+            dma((2, 15)),
+            dma((2, 6)),
+            dma((2, 6)),
+            dma((2, 3)),
+            dma((2, 3)),
+            dma((2, 3)),
+            dma((2, 3)),
         ],
         compiler_params=pltpu.CompilerParams(
-            collective_id=0, has_side_effects=True, vmem_limit_bytes=60 * 1024 * 1024
+            collective_id=0, has_side_effects=True, vmem_limit_bytes=24 * 1024 * 1024
         ),
-    )(tokens, lengths.reshape(1, 32), norm_gain, *weights, decay_base, rate_base, group_gain, state)
+    )(*operands)
+    updated = pltpu.with_memory_space_constraint(updated, pltpu.VMEM)
+    return pl.pallas_call(
+        flush,
+        out_shape=(
+            jax.ShapeDtypeStruct((32, 256), BF16),
+            jax.ShapeDtypeStruct(state.shape, F32),
+        ),
+        in_specs=[vmem, vmem],
+        out_specs=(vmem, anywhere),
+        scratch_shapes=[dma((2, 4))],
+        compiler_params=pltpu.CompilerParams(vmem_limit_bytes=1024 * 1024),
+    )(mixed, updated)
 
 
 def solution(mesh):

time: 103 us -> 80.9 us (0.79)
  the two profiles are of different devices: /device:TPU:0 before, /device:TPU:1 now
where the time goes in v2:
time: 80.9 us; the launch traced here: 80.8 us
  Pallas kernels  80.2 us (99%)
    pallas_call x1, Pallas kernels, local(): pl.pallas_call(kernel, out_shape=(jax.ShapeDtypeStruct((32, 256), BF16),...  76.2 us
    pallas_call x1, Pallas kernels, local(): pl.pallas_call(flush, out_shape=(jax.ShapeDtypeStruct((32, 256), BF16), j...  3.97 us

profile of v2, /device:TPU:1, one launch (start us, length us, event | category | flops | bytes accessed | tf_op | source)
XLA Modules:
  0.0 80.8 jit_solution(6898434219875351924)
XLA Ops:
  0.6 76.2 %shard_map.149 = (bf16[32,256]{1,0:T(8,128)(2,1)S(1)}, f32[2,32,4,64,64]{4,3,2,1,0:T(8,128)S(1)}) custom-call(bf16[32,256]{1,0:T(8,128)(2,1)} %tokens.1, s32[1,32]{1,0:T(1,128)} %bitcast.15, f32[2,4096]{1,0:T(2,128)} %norm_gain_hbm.1, bf16[2,32,4096]{2,1,0:T(8,128)(2,1)} %bitcast.8, bf16[2,32,4096]{2,1,0:T(8,128)(2,1)} %bitcast.9, ...), custom_call_target="tpu_custom_call" | custom-call | tf_op jit(solution)/shard_map/pallas_call | solution.py:508
  76.8 4.0 %shard_map.150 = (bf16[32,256]{1,0:T(8,128)(2,1)}, f32[2,32,4,64,64]{4,3,2,1,0:T(8,128)}) custom-call(bf16[32,256]{1,0:T(8,128)(2,1)S(1)} %get-tuple-element.4.mixed, f32[2,32,4,64,64]{4,3,2,1,0:T(8,128)S(1)} %get-tuple-element.5.updated), custom_call_target="tpu_custom_call" | custom-call | tf_op jit(solution)/shard_map/pallas_call | solution.py:555

commit v3 on v2

--- a/solution.py
+++ b/solution.py
@@ -13,7 +13,11 @@
 GROUP_EPS = 0.00064
 MESH = pl.DeviceIdType.MESH
 AXES = ("z", "y", "x")
-ORDERS = ((2, 1, 0), (1, 0, 2), (0, 2, 1), (1, 2, 0))
+PARTS = (
+    ((0, 24), (0, 128), (1, 2), 0),
+    ((0, 24), (128, 128), (0, 2), 1),
+    ((24, 8), (0, 256), (0, 1), 2),
+)
 PLANE = sorted(
     [(dz, dy) for dz in range(4) for dy in range(4) if dz or dy],
     key=lambda offset: -min(offset[0], 4 - offset[0]) - min(offset[1], 4 - offset[1]),
@@ -84,8 +88,8 @@
     def device(dim, step):
         return {AXES[dim]: peer(dim, step)}
 
-    def plane_device(dz, dy):
-        return {"z": peer(0, dz), "y": peer(1, dy)}
+    def plane_device(dims, one, two):
+        return {AXES[dims[0]]: peer(dims[0], one), AXES[dims[1]]: peer(dims[1], two)}
 
     sibling = {"core": 1 - core}
 
@@ -123,7 +127,9 @@
         return pltpu.make_async_copy(state.at[layer], st.at[layer], st_sem.at[layer])
 
     barrier = pltpu.get_barrier_semaphore()
-    partners = [device(2, step) for step in range(1, 4)] + [plane_device(*offset) for offset in PLANE] + [sibling]
+    partners = [device(dim, step) for dim in range(3) for step in range(1, 4)] + [sibling]
+    for dims in ((0, 1), (0, 2), (1, 2)):
+        partners += [plane_device(dims, *offset) for offset in PLANE if min(offset) > 0]
     for partner in partners:
         pl.semaphore_signal(barrier, inc=1, device_id=partner, device_id_type=MESH)
     for mat in range(6):
@@ -142,80 +148,76 @@
     ]
     for copy in small:
         copy.start()
-    pl.semaphore_wait(barrier, len(partners))
-
-    def region(buf, sub, sel):
-        where = tuple(pl.ds(start, size) for start, size in sel)
-        tile = (pl.ds(16 * (sub // 2), 16), pl.ds(128 * (sub % 2), 128))
-        return buf.at[where + tile]
-
-    def selection(parts):
-        return tuple(parts[dim] for dim in range(3))
-
-    def send(gid, buf, sub, stage, slot, sel, dim, step):
-        block = region(buf, sub, sel)
-        remote(block, block, g_send.at[gid, sub, stage], g_recv.at[gid, sub, slot], device(dim, step)).start()
-
-    def arrived(gid, buf, sub, slot, sel):
-        block = region(buf, sub, sel)
-        remote(block, block, g_send.at[gid, sub, 0], g_recv.at[gid, sub, slot], sibling).wait_recv()
-
-    def own_sel(dim_sel):
-        return selection([dim_sel.get(dim, (me[dim], 1)) for dim in range(3)])
-
-    def stage_one(gid, buf):
-        for step in (1, 3, 2):
-            for sub, (one, two, three) in enumerate(ORDERS):
-                send(gid, buf, sub, 0, step - 1, own_sel({}), one, step)
-
-    def stage_two(gid, buf):
-        for sub, (one, two, three) in enumerate(ORDERS):
-            for step in range(1, 4):
-                arrived(gid, buf, sub, step - 1, own_sel({one: (peer(one, 4 - step), 1)}))
-            for step in (1, 3, 2):
-                send(gid, buf, sub, 1, 2 + step, own_sel({one: (0, 4)}), two, step)
-
-    def stage_three(gid, buf):
-        for sub, (one, two, three) in enumerate(ORDERS):
-            for step in range(1, 4):
-                arrived(gid, buf, sub, 2 + step, own_sel({one: (0, 4), two: (peer(two, 4 - step), 1)}))
-            low = own_sel({one: (0, 2), two: (0, 4)})
-            high = own_sel({one: (2, 2), two: (0, 4)})
-            send(gid, buf, sub, 2, 6, low, three, 1)
-            send(gid, buf, sub, 2, 8, high, three, 3)
-            send(gid, buf, sub, 2, 7, high, three, 1)
-            send(gid, buf, sub, 2, 9, low, three, 3)
-
-    def stage_four(gid, buf):
-        for sub, (one, two, three) in enumerate(ORDERS):
-            low = own_sel({one: (0, 2), two: (0, 4), three: (peer(three, 3), 1)})
-            arrived(gid, buf, sub, 6, low)
-            send(gid, buf, sub, 2, 10, low, three, 1)
-            high = own_sel({one: (2, 2), two: (0, 4), three: (peer(three, 1), 1)})
-            arrived(gid, buf, sub, 8, high)
-            send(gid, buf, sub, 2, 11, high, three, 3)
-
-    def stage_five(gid, buf):
-        for sub, (one, two, three) in enumerate(ORDERS):
-            arrived(gid, buf, sub, 7, own_sel({one: (2, 2), two: (0, 4), three: (peer(three, 3), 1)}))
-            arrived(gid, buf, sub, 9, own_sel({one: (0, 2), two: (0, 4), three: (peer(three, 1), 1)}))
-            arrived(gid, buf, sub, 10, own_sel({one: (0, 2), two: (0, 4), three: (peer(three, 2), 1)}))
-            arrived(gid, buf, sub, 11, own_sel({one: (2, 2), two: (0, 4), three: (peer(three, 2), 1)}))
-
-    def gather_drain(gid, buf):
-        for sub, (one, two, three) in enumerate(ORDERS):
-            for stage, sel in enumerate(
-                ({one: (0, 3)}, {one: (0, 4), two: (0, 3)}, {one: (0, 4), two: (0, 4), three: (0, 3)})
-            ):
-                parts = selection([sel.get(dim, (0, 1)) for dim in range(3)])
-                block = region(buf, sub, parts)
-                remote(block, block, g_send.at[gid, sub, stage], g_recv.at[gid, sub, 0], sibling).wait_send()
+    with jax.named_scope("barrier"):
+        pl.semaphore_wait(barrier, len(partners))
+
+    def region(buf, part, sel):
+        rows, cols, _, _ = PARTS[part]
+        return buf.at[tuple(pl.ds(*sel[dim]) for dim in range(3)) + (pl.ds(*rows), pl.ds(*cols))]
+
+    def chosen(parts):
+        return [parts.get(dim, (me[dim], 1)) for dim in range(3)]
+
+    def send(gid, buf, part, stage, slot, sel, where):
+        block = region(buf, part, chosen(sel))
+        remote(block, block, g_send.at[gid, part, stage], g_recv.at[gid, part, slot], where).start()
+
+    def arrived(gid, buf, part, slot, sel):
+        block = region(buf, part, chosen(sel))
+        remote(block, block, g_send.at[gid, part, 0], g_recv.at[gid, part, slot], sibling).wait_recv()
+
+    def wide_one(gid, buf):
+        for one, two in PLANE:
+            for part, (_, _, dims, _) in enumerate(PARTS):
+                send(gid, buf, part, min(one, 1), 4 * one + two - 1, {}, plane_device(dims, one, two))
+
+    def halves(part, step):
+        _, _, dims, ring = PARTS[part]
+        place = {dims[1]: (0, 4)}
+        if step:
+            place[ring] = (peer(ring, step), 1)
+        return {**place, dims[0]: (0, 2)}, {**place, dims[0]: (2, 2)}
+
+    def wide_two(gid, buf):
+        for part, (_, _, dims, ring) in enumerate(PARTS):
+            for one, two in PLANE[::-1]:
+                place = {dims[0]: (peer(dims[0], 4 - one), 1), dims[1]: (peer(dims[1], 4 - two), 1)}
+                arrived(gid, buf, part, 4 * one + two - 1, place)
+            low, high = halves(part, 0)
+            send(gid, buf, part, 2, 15, low, device(ring, 1))
+            send(gid, buf, part, 2, 17, high, device(ring, 3))
+            send(gid, buf, part, 2, 16, high, device(ring, 1))
+            send(gid, buf, part, 2, 18, low, device(ring, 3))
+
+    def wide_three(gid, buf):
+        for part, (_, _, dims, ring) in enumerate(PARTS):
+            low, _ = halves(part, 3)
+            arrived(gid, buf, part, 15, low)
+            send(gid, buf, part, 2, 19, low, device(ring, 1))
+            _, high = halves(part, 1)
+            arrived(gid, buf, part, 17, high)
+            send(gid, buf, part, 2, 20, high, device(ring, 3))
+
+    def wide_four(gid, buf):
+        for part in range(3):
+            arrived(gid, buf, part, 16, halves(part, 3)[1])
+            arrived(gid, buf, part, 18, halves(part, 1)[0])
+        for part in range(3):
+            arrived(gid, buf, part, 19, halves(part, 2)[0])
+            arrived(gid, buf, part, 20, halves(part, 2)[1])
+
+    def wide_drain(gid, buf):
+        for part, (_, _, dims, ring) in enumerate(PARTS):
+            for stage, (one, two, three) in enumerate(((1, 3, 1), (3, 4, 1), (4, 4, 3))):
+                sel = {dims[0]: (0, one), dims[1]: (0, two), ring: (0, three)}
+                block = region(buf, part, chosen(sel))
+                remote(block, block, g_send.at[gid, part, stage], g_recv.at[gid, part, 0], sibling).wait_send()
 
     def plane_start(pid, buf):
         block = buf.at[me[0], me[1]]
         for dz, dy in PLANE:
             remote(
-                block, block, p_send.at[pid, min(dz, 1)], p_recv.at[pid, 4 * dz + dy - 1], plane_device(dz, dy)
+                block, block, p_send.at[pid, min(dz, 1)], p_recv.at[pid, 4 * dz + dy - 1], plane_device((0, 1), dz, dy)
             ).start()
 
     def plane_wait(pid, buf):
@@ -417,54 +419,56 @@
             sibling_weight(layer, mat).wait_send()
 
     scope = jax.named_scope
+    with scope("own"):
+        own.wait()
     with scope("g0_one"):
-        own.wait()
-        stage_one(0, g0)
+        wide_one(0, g0)
         for mat in range(6):
             sibling_weight(0, mat).start()
+        ring_start(0)
         state_in(0).start()
         start_weights(0, (6,))
     buffers = ((g0, g1), (g2, g3))
     for layer in range(2):
         wide, rows = buffers[layer]
         with scope("two"):
-            stage_two(layer, wide)
-        with scope("three"):
-            stage_three(layer, wide)
             if layer == 0:
                 for copy in small:
                     copy.wait()
+            wide_two(layer, wide)
+            if layer == 0:
                 start_weights(1, range(7))
                 state_in(1).start()
-        with scope("four"):
-            stage_four(layer, wide)
         with scope("scale"):
             weights_ready(layer, range(7))
             scale_weights(layer)
             drain_weights(layer)
-        with scope("five"):
-            stage_five(layer, wide)
+        with scope("three"):
+            wide_three(layer, wide)
+        with scope("four"):
+            wide_four(layer, wide)
         with scope("project"):
             project(layer, wide)
         with scope("exchange"):
             exchange(layer, a2a_s.at[layer], a2a_r.at[layer])
             a2a_r[layer, me[2]] = a2a_s[layer, me[2]]
-            gather_drain(layer, wide)
+            wide_drain(layer, wide)
             state_in(layer).wait()
             exchange_wait(layer, a2a_s.at[layer], a2a_r.at[layer])
-            ring_start(layer)
+        with scope("ring"):
+            ring_pass(layer)
+            ring_near(layer)
         with scope("recur"):
             rows[me[0], me[1]] = recur(layer)
         with scope("plane"):
             plane_start(layer, rows)
+            if layer == 0:
+                ring_start(1)
         with scope("update"):
             update_state(layer)
-        with scope("ring"):
-            ring_pass(layer)
-            exchange_drain(layer, a2a_s.at[layer], a2a_r.at[layer])
-            ring_near(layer)
         with scope("far"):
             ring_far(layer)
+            exchange_drain(layer, a2a_s.at[layer], a2a_r.at[layer])
         with scope("plane_wait"):
             plane_wait(layer, rows)
         with scope("ring_done"):
@@ -477,7 +481,7 @@
                 mixed_out[...] = result
         with scope("drain"):
             if layer == 0:
-                stage_one(1, g2)
+                wide_one(1, g2)
             plane_drain(layer, rows)
             ring_drain(layer)
 
@@ -536,8 +540,8 @@
             dma((2, 7)),
             dma((2, 7)),
             dma((2,)),
-            dma((2, 4, 3)),
-            dma((2, 4, 12)),
+            dma((2, 3, 3)),
+            dma((2, 3, 21)),
             dma((2, 2)),
             dma((2, 15)),
             dma((2, 6)),

time: 80.9 us -> 72.3 us (0.89)
  the two profiles are of different devices: /device:TPU:1 before, /device:TPU:0 now
where the time goes in v3:
time: 72.3 us; the launch traced here: 72.1 us
  Pallas kernels  71.5 us (99%)
    pallas_call x1, Pallas kernels, local(): pl.pallas_call(kernel, out_shape=(jax.ShapeDtypeStruct((32, 256), BF16),...  67.5 us
    pallas_call x1, Pallas kernels, local(): pl.pallas_call(flush, out_shape=(jax.ShapeDtypeStruct((32, 256), BF16), j...  3.97 us

profile of v3, /device:TPU:0, one launch (start us, length us, event | category | flops | bytes accessed | tf_op | source)
XLA Modules:
  0.0 72.1 jit_solution(16269980693716409818)
XLA Ops:
  0.6 67.5 %shard_map.149 = (bf16[32,256]{1,0:T(8,128)(2,1)S(1)}, f32[2,32,4,64,64]{4,3,2,1,0:T(8,128)S(1)}) custom-call(bf16[32,256]{1,0:T(8,128)(2,1)} %tokens.1, s32[1,32]{1,0:T(1,128)} %bitcast.15, f32[2,4096]{1,0:T(2,128)} %norm_gain_hbm.1, bf16[2,32,4096]{2,1,0:T(8,128)(2,1)} %bitcast.8, bf16[2,32,4096]{2,1,0:T(8,128)(2,1)} %bitcast.9, ...), custom_call_target="tpu_custom_call" | custom-call | tf_op jit(solution)/shard_map/pallas_call | solution.py:512
  68.2 4.0 %shard_map.150 = (bf16[32,256]{1,0:T(8,128)(2,1)}, f32[2,32,4,64,64]{4,3,2,1,0:T(8,128)}) custom-call(bf16[32,256]{1,0:T(8,128)(2,1)S(1)} %get-tuple-element.4.mixed, f32[2,32,4,64,64]{4,3,2,1,0:T(8,128)S(1)} %get-tuple-element.5.updated), custom_call_target="tpu_custom_call" | custom-call | tf_op jit(solution)/shard_map/pallas_call | solution.py:559
